TPU v7x, 32 devices: a whole 2x2x4 slice. The times are simulated.
32 devices in a mesh: dp: 4 (over y, x), kv: 4 (over z), tp: 2 (over core).
Axes of the slice: x: 2, y: 2, z: 4, core: 2. Of those that a mesh axis runs over, the one named last changes fastest.
Arguments:
- tokens: bfloat16 [24, 4096], P('dp', 'kv'), may hold values from -64 to 64
- lengths: int32 [24], P('dp'), may hold values from 128 to 1024, as said below
- attn_gain: float32 [4096], P('kv'), may hold values from 0.1 to 1.9
- query_weight: bfloat16 [4096, 4096], P('kv', 'tp'), may hold values from -0.09375 to 0.09375
- key_weight: bfloat16 [4096, 256], P('kv', 'tp'), may hold values from -0.1875 to 0.1875
- value_weight: bfloat16 [4096, 256], P('kv', 'tp'), may hold values from -0.09375 to 0.09375
- forget_weight: bfloat16 [4096, 4], replicated, may hold values from -0.25 to 0.25
- forget_offset: float32 [4], P('tp'), may hold values from -6 to 0
- cache_keys: bfloat16 [24, 1024, 256], P('dp', 'kv', 'tp'), may hold values from -1600 to 1600
- cache_values: bfloat16 [24, 1024, 256], P('dp', 'kv', 'tp'), may hold values from -6 to 6
- gate_sum: float32 [24, 4, 1024], P('dp', 'tp', 'kv'), may hold values from -82 to 0
- out_weight: bfloat16 [4096, 4096], P('tp', 'kv'), may hold values from -0.1875 to 0.1875
- mlp_gain: float32 [4096], replicated, may hold values from 0.1 to 1.9
- up_weight: bfloat16 [4096, 16384], P(None, ('kv', 'tp')), may hold values from -0.09375 to 0.09375
- down_weight: bfloat16 [16384, 4096], P(('kv', 'tp')), may hold values from -0.0625 to 0.0625
Outputs:
- mixed: bfloat16 [24, 4096], P('dp', ('kv', 'tp'))
Inputs may be any that keep to these rules, and one draw needn't show every extreme that they name: `lengths`: in every draw some sequence has all 1024 positions cached.
All inputs are finite; a program needn't handle non-finite values.
Results may differ from a plain program's by a relative error of at most 0.023.
Values may be sent and summed in bfloat16 or wider, within the bound.
A program may use at most 128 MiB of HBM per device.

v0:
```python
import jax
import jax.numpy as jnp
from jax import lax
from jax.sharding import PartitionSpec as P

D = 4096
HEADS = 64
HD = 64
KEY_VALUE_HEADS = 4
epsilon = 1e-06
floor_score = -1e30


def combined_all(x, axis, combine):
    everything = jax.tree.map(
        lambda part, kind: lax.all_gather(part.astype(kind), axis),
        x,
        (jnp.bfloat16, jnp.bfloat16, jnp.bfloat16),
    )

    def take(k):
        return jax.tree.map(lambda part, own: part[k].astype(own.dtype), everything, x)

    return lax.fori_loop(
        1, lax.axis_size(axis), lambda k, so_far: combine(so_far, take(k)), take(0)
    )


def combine_parts(earlier, later):
    first_top, first_total, first_values = earlier
    second_top, second_total, second_values = later
    merged_top = jnp.maximum(first_top, second_top)
    first_scale = jnp.exp(first_top - merged_top)
    second_scale = jnp.exp(second_top - merged_top)
    first_wide = jnp.repeat(first_scale, HD, axis=1)
    second_wide = jnp.repeat(second_scale, HD, axis=1)
    return (
        merged_top,
        first_total * first_scale + second_total * second_scale,
        first_values * first_wide + second_values * second_wide,
    )


def shards(
    tokens,
    lengths,
    attn_gain,
    query_weight,
    key_weight,
    value_weight,
    forget_weight,
    forget_offset,
    cache_keys,
    cache_values,
    gate_sum,
    out_weight,
    mlp_gain,
    up_weight,
    down_weight,
):
    row_count = tokens.shape[0]
    feature_cols = tokens.shape[1]
    kv_place = lax.axis_index("kv")
    tp_place = lax.axis_index("tp")
    local_heads = key_weight.shape[1] // HD
    group_size = HEADS // KEY_VALUE_HEADS
    token_rows = tokens.astype(jnp.float32)
    scaled_rows = (token_rows * attn_gain[None, :]).astype(jnp.bfloat16)
    square_part = jnp.sum(token_rows * token_rows, axis=1)
    query_part = jnp.dot(scaled_rows, query_weight, preferred_element_type=jnp.float32)
    key_part = jnp.dot(scaled_rows, key_weight, preferred_element_type=jnp.float32)
    value_part = jnp.dot(scaled_rows, value_weight, preferred_element_type=jnp.float32)
    gate_rows = lax.dynamic_slice(
        forget_weight,
        (kv_place * feature_cols, tp_place * local_heads),
        (feature_cols, local_heads),
    )
    forget_part = jnp.dot(scaled_rows, gate_rows, preferred_element_type=jnp.float32)
    query_sum, key_sum, value_sum, forget_sum, square_sum = lax.psum(
        (query_part, key_part, value_part, forget_part, square_part), "kv"
    )
    row_scale = lax.rsqrt(square_sum / D + epsilon)[:, None]
    queries = (query_sum * row_scale).astype(jnp.bfloat16)
    new_key = (key_sum * row_scale).astype(jnp.bfloat16)
    new_value = (value_sum * row_scale).astype(jnp.bfloat16)
    log_forget = jax.nn.log_sigmoid(forget_sum * row_scale + forget_offset[None, :])
    positions_here = cache_keys.shape[1]
    key_heads = cache_keys.reshape(row_count, positions_here, local_heads, HD)
    value_heads = cache_values.reshape(row_count, positions_here, local_heads, HD)
    query_heads = queries.reshape(row_count, local_heads, group_size, HD)
    scores = jnp.einsum(
        "skgd,spkd->skgp", query_heads, key_heads, preferred_element_type=jnp.float32
    ) * HD ** (-0.5)
    scores = scores + gate_sum[:, :, None, :] + log_forget[:, :, None, None]
    cache_pos = kv_place * positions_here + jnp.arange(positions_here)
    active_mask = (cache_pos[None, :] < lengths[:, None])[:, None, None, :]
    local_top = jnp.max(jnp.where(active_mask, scores, floor_score), axis=3)
    weights = jnp.where(active_mask, jnp.exp(scores - local_top[..., None]), 0.0)
    local_total = jnp.sum(weights, axis=3)
    local_values = jnp.einsum(
        "skgp,spkd->skgd",
        weights.astype(jnp.bfloat16),
        value_heads,
        preferred_element_type=jnp.float32,
    )
    head_cols = local_heads * group_size
    merged_top, merged_total, merged_values = combined_all(
        (
            local_top.reshape(row_count, head_cols),
            local_total.reshape(row_count, head_cols),
            local_values.reshape(row_count, head_cols * HD),
        ),
        "kv",
        combine_parts,
    )
    own_score = jnp.einsum(
        "skgd,skd->skg",
        query_heads,
        new_key.reshape(row_count, local_heads, HD),
        preferred_element_type=jnp.float32,
    ).reshape(row_count, head_cols) * HD ** (-0.5)
    final_top = jnp.maximum(merged_top, own_score)
    past_scale = jnp.exp(merged_top - final_top)
    own_weight = jnp.exp(own_score - final_top)
    totals = merged_total * past_scale + own_weight
    own_rounded = lax.optimization_barrier(own_weight.astype(jnp.bfloat16)).astype(jnp.float32)
    own_values = jnp.broadcast_to(
        new_value.astype(jnp.float32).reshape(row_count, local_heads, 1, HD),
        (row_count, local_heads, group_size, HD),
    ).reshape(row_count, head_cols * HD)
    weighted = (
        merged_values * jnp.repeat(past_scale, HD, axis=1)
        + jnp.repeat(own_rounded, HD, axis=1) * own_values
    )
    attended = (weighted / jnp.repeat(totals, HD, axis=1)).astype(jnp.bfloat16)
    partial_out = jnp.dot(attended, out_weight, preferred_element_type=jnp.float32)
    head_sum = lax.psum(partial_out.astype(jnp.bfloat16), "tp").astype(jnp.float32)
    mid_cols = (token_rows + head_sum).astype(jnp.bfloat16)
    mid_rows = lax.all_gather(mid_cols, "kv", axis=1, tiled=True)
    mid_wide = mid_rows.astype(jnp.float32)
    normed_mid = (
        mid_wide
        * mlp_gain[None, :]
        * lax.rsqrt(jnp.mean(mid_wide * mid_wide, axis=1, keepdims=True) + epsilon)
    ).astype(jnp.bfloat16)
    hidden = jnp.square(
        jax.nn.relu(jnp.dot(normed_mid, up_weight, preferred_element_type=jnp.float32))
    ).astype(jnp.bfloat16)
    mixer_term = jnp.dot(hidden, down_weight, preferred_element_type=jnp.float32)
    kv_count = lax.axis_size("kv")
    tp_count = lax.axis_size("tp")
    block_cols = mixer_term.shape[1] // (kv_count * tp_count)
    reordered = (
        mixer_term.reshape(row_count, kv_count, tp_count, block_cols)
        .transpose(0, 2, 1, 3)
        .reshape(row_count, kv_count * tp_count * block_cols)
    )
    pair_share = lax.psum_scatter(
        reordered.astype(jnp.bfloat16), "tp", scatter_dimension=1, tiled=True
    ).astype(jnp.float32)
    mixer_share = lax.psum_scatter(pair_share, "kv", scatter_dimension=1, tiled=True)
    out_cols = mixer_share.shape[1]
    start_col = (kv_place * tp_count + tp_place) * out_cols
    mid_share = lax.dynamic_slice_in_dim(mid_wide, start_col, out_cols, 1)
    return (mid_share + mixer_share).astype(jnp.bfloat16)


def solution(mesh):
    placed = (
        P("dp", "kv"),
        P("dp"),
        P("kv"),
        P("kv", "tp"),
        P("kv", "tp"),
        P("kv", "tp"),
        P(),
        P("tp"),
        P("dp", "kv", "tp"),
        P("dp", "kv", "tp"),
        P("dp", "tp", "kv"),
        P("tp", "kv"),
        P(),
        P(None, ("kv", "tp")),
        P(("kv", "tp"), None),
    )
    return jax.shard_map(
        shards, mesh=mesh, in_specs=placed, out_specs=P("dp", ("kv", "tp")), check_vma=False
    )
```

profile of v0, /device:TPU:0, one launch (start us, length us, event | category | flops | bytes accessed | tf_op | source)
XLA Modules:
  0.0 151.1 jit_solution(10252514063055072850)
XLA Ops:
  6.6 0.9 fusion.20
  7.4 2.9 %fusion.30 = f32[6,2048]{1,0:T(8,128)S(1)} fusion(bf16[1024,2048]{1,0:T(8,128)(2,1)} %param.20, bf16[6,1024]{1,0:T(8,128)(2,1)} %param.17, f32[1024]{0:T(1024)} %param.19), kind=kOutput, calls=%fused_computation.47 | convolution fusion | flops 25184256 | bytes 4259840 | tf_op jit(solution)/shard_map/dot_general | solution.py:70
  10.3 0.9 fusion.24
  11.2 1.1 fusion.26
  12.3 0.9 fusion.28
  13.3 22.1 %all-reduce = (f32[6,2048]{1,0:T(8,128)S(1)}, f32[6]{0:T(128)S(1)}, f32[6,128]{1,0:T(8,128)S(1)}, f32[6,2]{0,1:T(2,128)S(1)}, f32[6,128]{1,0:T(8,128)S(1)}) all-reduce(f32[6,2048]{1,0:T(8,128)S(1)} %fusion.30, f32[6]{0:T(128)S(1)} %fusion.20, f32[6,128]{1,0:T(8,128)S(1)} %fusion.26, ...), channel_id=1, replica_groups=mesh['dp'=4,'kv'=4,'tp'=2] {'kv'}, use_global_device_ids=true, to_apply=%region_0.0 | all-reduce | flops 13842 | bytes 110736 | tf_op jit(solution)/shard_map/psum | solution.py:79
  35.5 0.7 fusion.39
  36.4 1.2 copy.24
  37.5 1.2 copy.26
  38.7 0.7 broadcast_compare_fusion
  39.4 1.0 select_reduce_fusion
  41.0 13.6 %all_gather.17 = bf16[4,6,2048]{2,1,0:T(8,128)(2,1)S(1)} all-gather(bf16[1,6,2048]{2,1,0:T(8,128)(2,1)S(1)} %convert_element_type.173), channel_id=1, replica_groups=mesh['dp'=4,'kv'=4,'tp'=2] {'kv'}, dimensions={0}, use_global_device_ids=true | all-gather | bytes 122880 | tf_op jit(solution)/shard_map/all_gather | solution.py:16
  54.7 11.9 %all_gather.16 = bf16[4,6,32]{2,1,0:T(8,128)(2,1)S(1)} all-gather(bf16[1,6,32]{2,1,0:T(8,128)(2,1)S(1)} %convert_element_type.168), channel_id=1, replica_groups=mesh['dp'=4,'kv'=4,'tp'=2] {'kv'}, dimensions={0}, use_global_device_ids=true | all-gather | bytes 1920 | tf_op jit(solution)/shard_map/all_gather | solution.py:16
  66.7 11.9 %all_gather.15 = bf16[4,6,32]{2,1,0:T(8,128)(2,1)S(1)} all-gather(bf16[1,6,32]{2,1,0:T(8,128)(2,1)S(1)} %convert_element_type.164), channel_id=1, replica_groups=mesh['dp'=4,'kv'=4,'tp'=2] {'kv'}, dimensions={0}, use_global_device_ids=true | all-gather | bytes 1920 | tf_op jit(solution)/shard_map/all_gather | solution.py:16
  78.6 1.3 while.19
  81.1 2.8 %convolution_convert_fusion.2 = bf16[6,1024]{1,0:T(8,128)(2,1)S(1)} fusion(bf16[2048,1024]{1,0:T(8,128)(2,1)} %param.28, f32[6,2048]{1,0:T(8,128)S(1)} %reshape.150, f32[6,2048]{1,0:T(8,128)S(1)} %reshape.148, f32[6,2048]{1,0:T(8,128)S(1)} %reshape.149, f32[6,2048]{1,0:T(8,128)S(1)} %get-tuple-element.183, f32[6,2048]{1,0:T(8,128)S(1)} %reshape.147), kind=kOutput, calls=%fused_computation.16 | convolution fusion | flops 25233408 | bytes 4452352 | tf_op jit(solution)/shard_map/dot_general | solution.py:136
  83.9 3.4 %psum.47 = bf16[6,1024]{1,0:T(8,128)(2,1)S(1)} all-reduce(bf16[6,1024]{1,0:T(8,128)(2,1)S(1)} %convolution_convert_fusion.2), channel_id=1, replica_groups=mesh['dp'=4,'kv'=4,'tp'=2] {'tp'}, use_global_device_ids=true, to_apply=%region_10.11 | all-reduce | flops 6144 | bytes 24576 | tf_op jit(solution)/shard_map/psum | solution.py:137
  87.3 13.1 %all_gather.18 = bf16[6,4096]{1,0:T(8,128)(2,1)S(1)} all-gather(bf16[6,1024]{1,0:T(8,128)(2,1)S(1)} %fusion.21), channel_id=1, replica_groups=mesh['dp'=4,'kv'=4,'tp'=2] {'kv'}, dimensions={1}, use_global_device_ids=true | all-gather | bytes 61440 | tf_op jit(solution)/shard_map/all_gather | solution.py:139
  100.6 12.9 %convolution_convert_fusion = bf16[6,4096]{1,0:T(8,128)(2,1)S(1)} fusion(bf16[2048,4096]{1,0:T(8,128)(2,1)} %param.31, bf16[4096,2048]{1,0:T(8,128)(2,1)} %param.30, f32[6]{0:T(128)S(1)} %add_rsqrt_fusion, f32[4096]{0:T(1024)S(1)} %copy-done.2, bf16[6,4096]{1,0:T(8,128)(2,1)S(1)} %all_gather.18), kind=kOutput, calls=%fused_computation.8 | convolution fusion | flops 201486336 | bytes 33669144 | tf_op jit(solution)/shard_map/dot_general | solution.py:149
  113.6 0.7 convert_element_type.190
  114.3 5.9 %reduce-scatter.3.cloned.1.call-done = bf16[6,2048]{1,0:T(8,128)(2,1)} async-done(((bf16[6,4096]{1,0:T(8,128)(2,1)}), bf16[6,2048]{1,0:T(8,128)(2,1)}) %reduce-scatter.3.cloned.1.call-update) | async-done | bytes 24592 | tf_op jit(solution)/shard_map/reduce_scatter | solution.py:158
  120.2 1.4 convert_element_type.191
  121.6 21.3 %reduce-scatter.5.cloned.1.call-done = f32[6,512]{1,0:T(8,128)} async-done(((f32[6,2048]{1,0:T(8,128)}), f32[6,512]{1,0:T(8,128)}) %reduce-scatter.5.cloned.1.call-update) | async-done | bytes 12304 | tf_op jit(solution)/shard_map/reduce_scatter | solution.py:161
  142.9 1.3 add_convert_fusion
  (63 shorter events, 3.7 us)
Async XLA Ops:
  6.5 3.8 %copy-start = (bf16[1024,128]{1,0:T(8,128)(2,1)S(1)}, bf16[1024,128]{1,0:T(8,128)(2,1)}, u32[]{:S(2)}) copy-start(bf16[1024,128]{1,0:T(8,128)(2,1)} %param.22) | copy-start | bytes 786436
  6.5 80.7 %copy-start.1 = (bf16[6,1024]{1,0:T(8,128)(2,1)S(1)}, bf16[6,1024]{1,0:T(8,128)(2,1)}, u32[]{:S(2)}) copy-start(bf16[6,1024]{1,0:T(8,128)(2,1)} %param.17) | copy-start | bytes 36868
  6.5 94.1 %copy-start.2 = (f32[4096]{0:T(1024)S(1)}, f32[4096]{0:T(1024)}, u32[]{:S(2)}) copy-start(f32[4096]{0:T(1024)} %param.29) | copy-start | bytes 49156
  6.5 113.7 %reduce-scatter.3.cloned.1.call-start = ((), (), s32[]{:S(2)}) async-start(), calls=%async_computation.2 | async-start | bytes 98304 | tf_op jit(solution)/shard_map/reduce_scatter | solution.py:158
  114.3 28.6 %reduce-scatter.5.cloned.1.call-start = ((), (), s32[]{:S(2)}) async-start(), calls=%async_computation.3 | async-start | bytes 81920 | tf_op jit(solution)/shard_map/reduce_scatter | solution.py:161
Sparse Core Ops, SparseCore 0:
  114.4 5.7 reduce-scatter.2
  122.5 20.4 reduce-scatter.4
where the time goes:
time: 152 us; the launch traced here: 151 us
  blocking collectives  76 us (50%)
  waiting for transfers between devices  27.2 us (18%)
  matrix products  22.9 us (15%)
  between operations  13.6 us (9%)
  other arithmetic  5.77 us (4%)
  local copies, waits for them, and re-layouts  5.52 us (4%)
    all_gather x3, blocking collectives, combined_all(): lax.all_gather(part.astype(kind), axis)  37.4 us
    psum x1, blocking collectives, shards(): lax.psum((query_part, key_part, value_part, forget_part, square_part), 'kv')  22.1 us
    reduce_scatter x1, waiting for transfers between devices, shards(): lax.psum_scatter(pair_share, 'kv', scatter_dimension=1, tiled=True)  21.3 us
    all_gather x1, blocking collectives, shards(): mid_rows = lax.all_gather(mid_cols, 'kv', axis=1, tiled=True)  13.1 us
    dot_general x1, matrix products, shards(): jnp.dot(hidden, down_weight, preferred_element_type=jnp.float32)  12.9 us
    reduce_scatter x1, waiting for transfers between devices, shards(): lax.psum_scatter(reordered.astype(jnp.bfloat16), 'tp', scatter_dimension=...  5.88 us
    psum x1, blocking collectives, shards(): lax.psum(partial_out.astype(jnp.bfloat16), 'tp').astype(jnp.float32)  3.36 us
  transfers between devices with their start and end apart: 2, of which 2 were waited for; matrix products, arithmetic and copies ran while one was open for 0% of the time, Pallas kernels for 0%

commit v1 on v0

--- a/solution.py
+++ b/solution.py
@@ -9,6 +9,28 @@
 KEY_VALUE_HEADS = 4
 epsilon = 1e-06
 floor_score = -1e30
+
+
+def in_order(blocks, dim):
+    shape = list(blocks.shape[1:])
+    shape[dim] *= blocks.shape[0]
+    return jnp.moveaxis(blocks, 0, dim).reshape(shape)
+
+
+def gather_around(array, axis, dim):
+    length = lax.axis_size(axis)
+    pairs = [(i, (i + 1) % length) for i in range(length)]
+    back = [(b, a) for a, b in pairs]
+    lower, upper = ([], [])
+    for lap in range(length - 1):
+        if lap % 2 == 0:
+            lower.append(lax.ppermute(lower[-1] if lower else array, axis, pairs))
+        else:
+            upper.append(lax.ppermute(upper[-1] if upper else array, axis, back))
+    blocks = jnp.stack([*lower[::-1], array, *upper])
+    shift = lax.axis_index(axis) - len(lower)
+    blocks = blocks[(jnp.arange(length) - shift) % length]
+    return in_order(blocks, dim)
 
 
 def combined_all(x, axis, combine):
@@ -136,7 +158,7 @@
     partial_out = jnp.dot(attended, out_weight, preferred_element_type=jnp.float32)
     head_sum = lax.psum(partial_out.astype(jnp.bfloat16), "tp").astype(jnp.float32)
     mid_cols = (token_rows + head_sum).astype(jnp.bfloat16)
-    mid_rows = lax.all_gather(mid_cols, "kv", axis=1, tiled=True)
+    mid_rows = gather_around(mid_cols, "kv", 1)
     mid_wide = mid_rows.astype(jnp.float32)
     normed_mid = (
         mid_wide

time: 152 us -> 150 us (0.987)
  blocking collectives: 76 us -> 62.8 us
  waiting for transfers between devices: 27.2 us -> 34.4 us
  starting transfers between devices: 0.04 us -> 3.92 us
    all_gather x1 -> x0, blocking collectives: 13.1 us -> none  [shards(): mid_rows = lax.all_gather(mid_cols, 'kv', axis=1, tiled=True)]
    ppermute x0 -> x3, waiting for transfers between devices: none -> 7.22 us  [the longest x2 7.21 us: gather_around(): lower.append(lax.ppermute(lower[-1] if lower else array, axis, pairs))]
    ppermute x0 -> x3, starting transfers between devices: none -> 3.87 us  [the longest x1 3.81 us: gather_around(): upper.append(lax.ppermute(upper[-1] if upper else array, axis, back))]
  transfers between devices with their start and end apart: 2 -> 5, of which waited for: 2 -> 4; matrix products, arithmetic and copies ran while one was open for 0% -> 0% of each run, Pallas kernels for 0% -> 0%
where the time goes in v1:
time: 150 us
  blocking collectives  62.8 us (42%)
  waiting for transfers between devices  34.4 us (23%)
  matrix products  22.9 us (15%)
  between operations  13.6 us (9%)
  local copies, waits for them, and re-layouts  6.07 us (4%)
  other arithmetic  5.81 us (4%)
  starting transfers between devices  3.92 us (3%)
    all_gather x3, blocking collectives, combined_all(): lax.all_gather(part.astype(kind), axis)  37.4 us
    psum x1, blocking collectives, shards(): lax.psum((query_part, key_part, value_part, forget_part, square_part), 'kv')  22.1 us
    reduce_scatter x1, waiting for transfers between devices, shards(): lax.psum_scatter(pair_share, 'kv', scatter_dimension=1, tiled=True)  21.3 us
    dot_general x1, matrix products, shards(): jnp.dot(hidden, down_weight, preferred_element_type=jnp.float32)  12.9 us
    ppermute x2, waiting for transfers between devices, gather_around(): lower.append(lax.ppermute(lower[-1] if lower else array, axis, pairs))  7.21 us
    reduce_scatter x1, waiting for transfers between devices, shards(): lax.psum_scatter(reordered.astype(jnp.bfloat16), 'tp', scatter_dimension=...  5.85 us
    ppermute x1, starting transfers between devices, gather_around(): upper.append(lax.ppermute(upper[-1] if upper else array, axis, back))  3.81 us
    psum x1, blocking collectives, shards(): lax.psum(partial_out.astype(jnp.bfloat16), 'tp').astype(jnp.float32)  3.36 us
  transfers between devices with their start and end apart: 5, of which 4 were waited for; matrix products, arithmetic and copies ran while one was open for 0% of the time, Pallas kernels for 0%

profile of v1, /device:TPU:0, one launch (start us, length us, event | category | flops | bytes accessed | tf_op | source)
XLA Modules:
  0.0 149.6 jit_solution(17419905353608560941)
XLA Ops:
  6.6 0.9 fusion.18
  7.4 2.9 %fusion.28 = f32[6,2048]{1,0:T(8,128)S(1)} fusion(bf16[1024,2048]{1,0:T(8,128)(2,1)} %param.20, bf16[6,1024]{1,0:T(8,128)(2,1)} %param.17, f32[1024]{0:T(1024)} %param.19), kind=kOutput, calls=%fused_computation.47 | convolution fusion | flops 25184256 | bytes 4259840 | tf_op jit(solution)/shard_map/dot_general | solution.py:92
  10.3 0.9 fusion.22
  11.2 1.1 fusion.24
  12.3 0.9 fusion.26
  13.3 22.1 %all-reduce = (f32[6,2048]{1,0:T(8,128)S(1)}, f32[6]{0:T(128)S(1)}, f32[6,128]{1,0:T(8,128)S(1)}, f32[6,2]{0,1:T(2,128)S(1)}, f32[6,128]{1,0:T(8,128)S(1)}) all-reduce(f32[6,2048]{1,0:T(8,128)S(1)} %fusion.28, f32[6]{0:T(128)S(1)} %fusion.18, f32[6,128]{1,0:T(8,128)S(1)} %fusion.24, ...), channel_id=1, replica_groups=mesh['dp'=4,'kv'=4,'tp'=2] {'kv'}, use_global_device_ids=true, to_apply=%region_0.0 | all-reduce | flops 13842 | bytes 110736 | tf_op jit(solution)/shard_map/psum | solution.py:101
  35.5 0.7 fusion.37
  36.4 1.2 copy.24
  37.5 1.2 copy.26
  39.4 1.0 select_reduce_fusion
  41.0 13.6 %all_gather.14 = bf16[4,6,2048]{2,1,0:T(8,128)(2,1)S(1)} all-gather(bf16[1,6,2048]{2,1,0:T(8,128)(2,1)S(1)} %convert_element_type.183), channel_id=1, replica_groups=mesh['dp'=4,'kv'=4,'tp'=2] {'kv'}, dimensions={0}, use_global_device_ids=true | all-gather | bytes 122880 | tf_op jit(solution)/shard_map/all_gather | solution.py:38
  54.7 11.9 %all_gather.13 = bf16[4,6,32]{2,1,0:T(8,128)(2,1)S(1)} all-gather(bf16[1,6,32]{2,1,0:T(8,128)(2,1)S(1)} %convert_element_type.178), channel_id=1, replica_groups=mesh['dp'=4,'kv'=4,'tp'=2] {'kv'}, dimensions={0}, use_global_device_ids=true | all-gather | bytes 1920 | tf_op jit(solution)/shard_map/all_gather | solution.py:38
  66.7 11.9 %all_gather.12 = bf16[4,6,32]{2,1,0:T(8,128)(2,1)S(1)} all-gather(bf16[1,6,32]{2,1,0:T(8,128)(2,1)S(1)} %convert_element_type.174), channel_id=1, replica_groups=mesh['dp'=4,'kv'=4,'tp'=2] {'kv'}, dimensions={0}, use_global_device_ids=true | all-gather | bytes 1920 | tf_op jit(solution)/shard_map/all_gather | solution.py:38
  78.6 1.3 while.19
  81.1 2.8 %convolution_convert_fusion.2 = bf16[6,1024]{1,0:T(8,128)(2,1)S(1)} fusion(bf16[2048,1024]{1,0:T(8,128)(2,1)} %param.28, f32[6,2048]{1,0:T(8,128)S(1)} %reshape.202, f32[6,2048]{1,0:T(8,128)S(1)} %reshape.200, f32[6,2048]{1,0:T(8,128)S(1)} %reshape.201, f32[6,2048]{1,0:T(8,128)S(1)} %get-tuple-element.183, f32[6,2048]{1,0:T(8,128)S(1)} %reshape.199), kind=kOutput, calls=%fused_computation.17 | convolution fusion | flops 25233408 | bytes 4452352 | tf_op jit(solution)/shard_map/dot_general | solution.py:158
  83.9 3.4 %psum.47 = bf16[6,1024]{1,0:T(8,128)(2,1)S(1)} all-reduce(bf16[6,1024]{1,0:T(8,128)(2,1)S(1)} %convolution_convert_fusion.2), channel_id=1, replica_groups=mesh['dp'=4,'kv'=4,'tp'=2] {'tp'}, use_global_device_ids=true, to_apply=%region_10.11 | all-reduce | flops 6144 | bytes 24576 | tf_op jit(solution)/shard_map/psum | solution.py:159
  87.4 3.8 %collective-permute-start.2 = (bf16[6,1024]{1,0:T(8,128)(2,1)S(1)}, bf16[6,1024]{1,0:T(8,128)(2,1)S(1)}, u32[]{:S(2)}, u32[]{:S(2)}) collective-permute-start(bf16[6,1024]{1,0:T(8,128)(2,1)S(1)} %fusion.19), channel_id=1, source_target_pairs={{2,0},{4,2},{6,4},{0,6},{3,1},{5,3},{7,5},{1,7},{10,8},{12,10},{14... | collective-permute-start | bytes 36872 | tf_op jit(solution)/shard_map/ppermute | solution.py:29
  91.2 1.7 %collective-permute-done = bf16[6,1024]{1,0:T(8,128)(2,1)S(1)} collective-permute-done((bf16[6,1024]{1,0:T(8,128)(2,1)S(1)}, bf16[6,1024]{1,0:T(8,128)(2,1)S(1)}, u32[]{:S(2)}, u32[]{:S(2)}) %collective-permute-start) | collective-permute-done | bytes 12320 | tf_op jit(solution)/shard_map/ppermute | solution.py:27
  92.9 5.5 %collective-permute-done.1 = bf16[6,1024]{1,0:T(8,128)(2,1)S(1)} collective-permute-done((bf16[6,1024]{1,0:T(8,128)(2,1)S(1)}, bf16[6,1024]{1,0:T(8,128)(2,1)S(1)}, u32[]{:S(2)}, u32[]{:S(2)}) %collective-permute-start.1) | collective-permute-done | bytes 12320 | tf_op jit(solution)/shard_map/ppermute | solution.py:27
  99.2 12.9 %convolution_convert_fusion = bf16[6,4096]{1,0:T(8,128)(2,1)S(1)} fusion(bf16[2048,4096]{1,0:T(8,128)(2,1)} %param.31, bf16[4096,2048]{1,0:T(8,128)(2,1)} %param.30, f32[6,4096]{1,0:T(8,128)S(1)} %bitcast.61, f32[6]{0:T(128)S(1)} %add_rsqrt_fusion, f32[4096]{0:T(1024)S(1)} %copy-done.2), kind=kOutput, calls=%fused_computation.9 | convolution fusion | flops 201461760 | bytes 33718296 | tf_op jit(solution)/shard_map/dot_general | solution.py:171
  112.9 5.9 %reduce-scatter.3.cloned.1.call-done = bf16[6,2048]{1,0:T(8,128)(2,1)} async-done(((bf16[6,4096]{1,0:T(8,128)(2,1)}), bf16[6,2048]{1,0:T(8,128)(2,1)}) %reduce-scatter.3.cloned.1.call-update) | async-done | bytes 24592 | tf_op jit(solution)/shard_map/reduce_scatter | solution.py:180
  118.8 1.4 convert_element_type.204
  120.2 21.3 %reduce-scatter.5.cloned.1.call-done = f32[6,512]{1,0:T(8,128)} async-done(((f32[6,2048]{1,0:T(8,128)}), f32[6,512]{1,0:T(8,128)}) %reduce-scatter.5.cloned.1.call-update) | async-done | bytes 12304 | tf_op jit(solution)/shard_map/reduce_scatter | solution.py:183
  141.5 1.3 add_convert_fusion
  (72 shorter events, 5.7 us)
Async XLA Ops:
  6.5 3.8 %copy-start = (bf16[1024,128]{1,0:T(8,128)(2,1)S(1)}, bf16[1024,128]{1,0:T(8,128)(2,1)}, u32[]{:S(2)}) copy-start(bf16[1024,128]{1,0:T(8,128)(2,1)} %param.22) | copy-start | bytes 786436
  6.5 80.7 %copy-start.1 = (bf16[6,1024]{1,0:T(8,128)(2,1)S(1)}, bf16[6,1024]{1,0:T(8,128)(2,1)}, u32[]{:S(2)}) copy-start(bf16[6,1024]{1,0:T(8,128)(2,1)} %param.17) | copy-start | bytes 36868
  6.5 92.7 %copy-start.2 = (f32[4096]{0:T(1024)S(1)}, f32[4096]{0:T(1024)}, u32[]{:S(2)}) copy-start(f32[4096]{0:T(1024)} %param.29) | copy-start | bytes 49156
  6.5 112.2 %reduce-scatter.3.cloned.1.call-start = ((), (), s32[]{:S(2)}) async-start(), calls=%async_computation.2 | async-start | bytes 98304 | tf_op jit(solution)/shard_map/reduce_scatter | solution.py:180
  87.3 5.6 %collective-permute-start = (bf16[6,1024]{1,0:T(8,128)(2,1)S(1)}, bf16[6,1024]{1,0:T(8,128)(2,1)S(1)}, u32[]{:S(2)}, u32[]{:S(2)}) collective-permute-start(bf16[6,1024]{1,0:T(8,128)(2,1)S(1)} %fusion.19), channel_id=1, source_target_pairs={{0,2},{2,4},{4,6},{6,0},{1,3},{3,5},{5,7},{7,1},{8,10},{10,12},{12... | collective-permute-start | bytes 36872 | tf_op jit(solution)/shard_map/ppermute | solution.py:27
  87.4 5.5 %collective-permute-start.2 = (bf16[6,1024]{1,0:T(8,128)(2,1)S(1)}, bf16[6,1024]{1,0:T(8,128)(2,1)S(1)}, u32[]{:S(2)}, u32[]{:S(2)}) collective-permute-start(bf16[6,1024]{1,0:T(8,128)(2,1)S(1)} %fusion.19), channel_id=1, source_target_pairs={{2,0},{4,2},{6,4},{0,6},{3,1},{5,3},{7,5},{1,7},{10,8},{12,10},{14... | collective-permute-start | bytes 36872 | tf_op jit(solution)/shard_map/ppermute | solution.py:29
  92.9 5.5 %collective-permute-start.1 = (bf16[6,1024]{1,0:T(8,128)(2,1)S(1)}, bf16[6,1024]{1,0:T(8,128)(2,1)S(1)}, u32[]{:S(2)}, u32[]{:S(2)}) collective-permute-start(bf16[6,1024]{1,0:T(8,128)(2,1)S(1)} %collective-permute-done), channel_id=1, source_target_pairs={{0,2},{2,4},{4,6},{6,0},{1,3},{3,5},{5,7},{7,1},{8,10},{10,12},{12... | collective-permute-start | bytes 36872 | tf_op jit(solution)/shard_map/ppermute | solution.py:27
  112.9 28.6 %reduce-scatter.5.cloned.1.call-start = ((), (), s32[]{:S(2)}) async-start(), calls=%async_computation.3 | async-start | bytes 81920 | tf_op jit(solution)/shard_map/reduce_scatter | solution.py:183
Sparse Core Ops, SparseCore 0:
  113.0 5.7 reduce-scatter.2
  121.0 20.4 reduce-scatter.4
